TPU v7x, 32 devices: a whole 2x2x4 slice. The times are simulated.
32 devices in a mesh: rep: 16 (over z, y, core), fs: 2 (over x), tp: 1.
Axes of the slice: x: 2, y: 2, z: 4, core: 2. Of those that a mesh axis runs over, the one named last changes fastest.
Arguments:
- pre_act: bfloat16 [16384, 4096], P('rep', ('fs', 'tp')), may hold values from -6 to 6
- down_weight: bfloat16 [4096, 2048], P(('fs', 'tp')), may hold values from -0.09375 to 0.09375
- cotangent: bfloat16 [16384, 2048], P('rep', ('fs', 'tp')), may hold values from -6 to 6
Outputs:
- grad_pre: bfloat16 [16384, 4096], P('rep', ('fs', 'tp'))
- grad_weight: float32 [4096, 2048], P(('fs', 'tp', 'rep'))
All inputs are finite; a program needn't handle non-finite values.
Results may differ from a plain program's by a relative error of at most 0.0029.
Values may be sent and summed in bfloat16 or wider, within the bound.
A program may use at most 128 MiB of HBM per device.

v0:
```python
import functools

import jax
import jax.numpy as jnp
from jax import lax
from jax.experimental import pallas as pl
from jax.experimental.pallas import tpu as pltpu
from jax.sharding import PartitionSpec as P

MESH = pl.DeviceIdType.MESH
CORES, ROWS = 2, 2
F32, BF16 = jnp.float32, jnp.bfloat16


ORDER = (
    "n0 A0 n1 A1",
    "o4 i4 B0 B1",
    "n2 A2 n3 A3",
    "s0 B2 x0 B3",
    "f0 A4 B4 s1",
    "g0 g1 t0 g2",
    "x1 s2 f1 A5",
    "B5 g3 t1 h0",
    "h1 s3 h2 t2",
    "h3 x2 s4 l0",
    "f2 A6 B6 t3",
    "s5 l1 x3 t4",
    "f3 A7 B7 t5",
    "l2 x4 s6 f4",
    "A8 B8 s7 e0",
    "t6 l3 e1 s8",
    "l4 e2 l5 e3",
    "l6 l7 l8",
)


def chunks_of(width, sizes):
    out, at = [], 0
    for s in sizes:
        out.append((at, s))
        at += s
    assert at == width
    return out


def plain(pre_act, down_weight, cotangent):
    whole = lax.all_gather(cotangent, ("fs", "tp"), axis=1, tiled=True)
    grad_hidden = lax.dot_general(
        whole, down_weight, (((1,), (1,)), ((), ())), preferred_element_type=F32
    )
    positive = jnp.maximum(pre_act.astype(F32), 0.0)
    grad_pre = (grad_hidden * 2.0 * positive).astype(BF16)
    hidden = (positive * positive).astype(BF16)
    factor = 1.0 / jnp.sqrt(jnp.float32(pre_act.shape[0] * lax.axis_size("rep")))
    term = lax.dot_general(
        hidden, whole, (((0,), (0,)), ((), ())), preferred_element_type=F32
    )
    summed = lax.psum_scatter(term, "rep", scatter_dimension=0, tiled=True)
    return (grad_pre, summed * factor)


def kernel(
    depth, near, far, most, order, factor,
    pre_hbm, w_hbm, cot_hbm, gp, gw,
    pre, pre_in, turned, w, cot, grad,
    y_out, y_in, own, z_out, z_in,
    s_local, s_pre_s, s_pre_r, s_near_s, s_near_r, s_x_s, s_x_r, s_fwd_s, s_fwd_r,
    s_y_s, s_y_r, s_z_s, s_z_r,
):
    rep, fs, tp = lax.axis_index("rep"), lax.axis_index("fs"), lax.axis_index("tp")
    c, y, z = rep % CORES, (rep // CORES) % ROWS, rep // (CORES * ROWS)
    tokens, half = cot_hbm.shape
    hid = w_hbm.shape[0]
    block = own.shape[1]
    blocks = 2 * depth

    def at(z_, y_, c_, f_):
        return ((z_ * ROWS + y_) * CORES + c_, f_, tp)

    partner, across, beside = at(z, y, 1 - c, fs), at(z, y, c, 1 - fs), at(z, 1 - y, c, fs)

    def remote(src, dst, s, r, to):
        return pltpu.make_async_remote_copy(
            src_ref=src, dst_ref=dst, send_sem=s, recv_sem=r, device_id=to, device_id_type=MESH
        )

    def columns(i, c_):
        y_ = (1 - y) if i < depth else y
        k = (i % depth) * ROWS + y_
        return pl.ds(pl.multiple_of((k * CORES + c_) * block, block), block)

    def local(i, src, dst):
        return pltpu.make_async_copy(src, dst, s_local.at[i])

    loads = [local(0, pre_hbm, pre), local(1, cot_hbm, cot.at[0, pl.ds(0, tokens)]), local(2, w_hbm, w)]
    for l in loads:
        l.start()

    barrier = pltpu.get_barrier_semaphore()
    peers = [partner, across, beside]
    for d in range(1, depth):
        peers.append(at((z + d) % depth, y, c, fs))
    for p in peers:
        pl.semaphore_signal(barrier, inc=1, device_id=p, device_id_type=MESH)
    pl.semaphore_wait(barrier, len(peers))

    x_copies = []
    for q, (a, n) in enumerate(far):
        x_copies.append(remote(
            cot_hbm.at[:, pl.ds(a, n)], cot.at[1, pl.ds(0, tokens), pl.ds(a, n)],
            s_x_s.at[q], s_x_r.at[q], across))
    x_copies[0].start()
    pre_copies = []
    for i in range(blocks):
        pre_copies.append(remote(
            pre_hbm.at[:, columns(i, 1 - c)], pre_in.at[i], s_pre_s.at[i], s_pre_r.at[i], partner))
    near_copies = []
    for q, (a, n) in enumerate(near):
        near_copies.append(remote(
            cot_hbm.at[:, pl.ds(a, n)], cot.at[0, pl.ds(tokens, tokens), pl.ds(a, n)],
            s_near_s.at[q], s_near_r.at[q], partner))
    for group in (pre_copies[:depth], near_copies[:2], pre_copies[depth:], near_copies[2:]):
        for copy in group:
            copy.start()
    for xc in x_copies[1:]:
        xc.start()

    def turn(v):
        p = jnp.maximum(v.astype(F32), 0.0)
        return (p * p).T.astype(BF16)

    strip = 256

    def turn_own(first):
        for i in range(first, first + depth):
            cols = columns(i, c)

            @pl.loop(0, tokens // strip)
            def _(t):
                rows = pl.ds(pl.multiple_of(t * strip, strip), strip)
                turned[pl.ds(i * block, block), rows] = turn(pre[rows, cols])

    def turn_in(first):
        for i in range(first, first + depth):
            pre_copies[i].wait_recv()

        @pl.loop(first, first + depth)
        def _(i):
            @pl.loop(0, tokens // strip)
            def _(t):
                rows = pl.ds(pl.multiple_of(t * strip, strip), strip)
                to = pl.ds(pl.multiple_of(tokens + t * strip, strip), strip)
                turned[pl.ds(pl.multiple_of(i * block, block), block), to] = turn(pre_in[i, rows, :])

    tall = 2 * block

    chunks = [(0, a, n) for a, n in near] + [(1, a, n) for a, n in far]

    def span(h, a, n):
        return pl.ds(h * half + a, n)

    def y_copy(j):
        h, a, n = chunks[j]
        s = span(h, a, n)
        return remote(y_out.at[:, :, s], y_in.at[:, :, s], s_y_s.at[j], s_y_r.at[j], beside)

    slots, far_end = depth, depth - 1
    inner = (z > 0) & (z < far_end)

    def relayed(j):
        return j < len(chunks) - 2

    def z_copy(j, kind):
        h, a, n = chunks[j]
        s = span(h, a, n)
        if kind == "up":
            ends = (z == far_end) if relayed(j) else False
            block_, slot, to = jnp.where(ends, 0, (z + 1) % depth), jnp.where(ends, 3, 0), jnp.where(ends, far_end - 1, (z + 1) % depth)
        elif kind == "down":
            ends = (z == 0) if relayed(j) else False
            block_, slot, to = jnp.where(ends, far_end, (z + far_end) % depth), jnp.where(ends, 3, 2), jnp.where(ends, 1, (z + far_end) % depth)
        else:
            block_, slot, to = (z + 2) % depth, 1, (z + 2) % depth
        return remote(
            z_out.at[block_, :, s], z_in.at[slot, :, s],
            s_z_s.at[j * slots + slot], s_z_r.at[j * slots + slot], at(to, y, c, fs))

    def z_arrival(j, slot):
        h, a, n = chunks[j]
        s = span(h, a, n)
        return remote(
            z_out.at[0, :, s], z_in.at[slot, :, s],
            s_z_s.at[j * slots + slot], s_z_r.at[j * slots + slot], beside)

    def fwd_copy(q):
        a, n = far[q]
        return remote(
            cot.at[1, pl.ds(0, tokens), pl.ds(a, n)], cot.at[1, pl.ds(tokens, tokens), pl.ds(a, n)],
            s_fwd_s.at[q], s_fwd_r.at[q], partner)

    def product(j, mine):
        h, a, n = chunks[j]
        s = span(h, a, n)

        def dot(m):
            rows = pl.ds(pl.multiple_of(m * tall, tall), tall)
            return lax.dot_general(
                turned[rows, :], cot[h, :, pl.ds(a, n)], (((1,), (0,)), ((), ())),
                preferred_element_type=F32).reshape(2, block, n)

        if mine:

            @pl.loop(0, depth // 2)
            def _(m):
                own[pl.ds(m * 2, 2), :, s] = dot(m + depth // 2)
        else:

            @pl.loop(0, depth // 2)
            def _(m):
                y_out[pl.ds(m * 2, 2), :, s] = dot(m).astype(BF16)

            y_copy(j).start()

    def second(j):
        h, a, n = chunks[j]
        s = span(h, a, n)
        y_copy(j).wait_recv()

        @pl.loop(0, depth)
        def _(k):
            v = own[k, :, s] + y_in[k, :, s].astype(F32)
            own[k, :, s] = v
            z_out[k, :, s] = v.astype(BF16)

        z_copy(j, "up").start()
        z_copy(j, "down").start()

        if relayed(j):

            @pl.when(jnp.logical_not(inner))
            def _():
                z_copy(j, "two").start()
        else:
            z_copy(j, "two").start()

    def third(j):
        h, a, n = chunks[j]
        s = span(h, a, n)

        @pl.when(inner)
        def _():
            z_arrival(j, 3).wait_recv()
            to = (z + 2) % depth
            z_out[to, :, s] = (own[to, :, s] + z_in[3, :, s].astype(F32)).astype(BF16)
            z_copy(j, "two").start()

    def last(j):
        h, a, n = chunks[j]
        s = span(h, a, n)
        for slot, there in ((0, z > 0), (2, z < far_end), (1, None)) if relayed(j) else ((0, None), (2, None), (1, None)):

            def add(slot=slot):
                z_arrival(j, slot).wait_recv()
                own[z, :, s] = own[z, :, s] + z_in[slot, :, s].astype(F32)

            if there is None:
                add()
            else:
                pl.when(there)(add)
        place = pl.multiple_of((fs if h == 0 else 1 - fs) * half + a, 128)
        gw[:, pl.ds(place, n)] = own[z, :, s] * factor

    tm, tn = 256, 512

    def grad_tile(h, a, n, m, k):
        rows = pl.ds(pl.multiple_of(m * tm, tm), tm)
        outs = pl.ds(pl.multiple_of(k * tn, tn), tn)
        place = pl.multiple_of((fs if h == 0 else 1 - fs) * half + a, 128)
        return rows, outs, lax.dot_general(
            cot[h, rows, pl.ds(a, n)], w[outs, pl.ds(place, n)], (((1,), (1,)), ((), ())),
            preferred_element_type=F32)

    def grad_first(m):
        if m == 0:
            loads[2].wait()

        @pl.loop(0, hid // tn)
        def _(k):
            rows, outs, v = grad_tile(0, 0, half, m, k)
            grad[rows, outs] = v

    def grad_next(m):
        @pl.loop(0, hid // tn)
        def _(k):
            rows, outs, v = grad_tile(1, 0, most, m, k)
            grad[rows, outs] += v

    def grad_rest(m):
        @pl.loop(0, hid // tn)
        def _(k):
            rows, outs, v = grad_tile(1, most, half - most, m, k)
            p = jnp.maximum(pre[rows, outs].astype(F32), 0.0)
            gp[rows, outs] = ((grad[rows, outs] + v) * 2.0 * p).astype(BF16)

    def near_in(q):
        near_copies[q].wait_recv()

    def far_in(q):
        x_copies[q].wait_recv()
        fwd_copy(q).start()

    def far_both(q):
        fwd_copy(q).wait_recv()

    nn, nf = len(near), len(far)
    total = nn + nf
    steps = {
        "A": lambda j: product(j, False), "B": lambda j: product(j, True),
        "s": second, "t": third, "l": last, "n": near_in, "x": far_in, "f": far_both,
        "g": grad_first, "h": grad_next, "e": grad_rest, "o": turn_own, "i": turn_in,
    }
    loads[0].wait()
    turn_own(0)
    loads[1].wait()
    turn_in(0)
    for step in " ".join(order).split():
        steps[step[0]](int(step[1:]))

    for copy in pre_copies + near_copies + x_copies:
        copy.wait_send()
    for q in range(nf):
        fwd_copy(q).wait_send()
    for j in range(total):
        y_copy(j).wait_send()
        for kind in ("up", "down", "two"):
            z_copy(j, kind).wait_send()


def solution(mesh):
    reps, fs, tp = mesh.shape["rep"], mesh.shape["fs"], mesh.shape["tp"]
    depth = reps // (CORES * ROWS)

    def on_device(pre_act, down_weight, cotangent):
        tokens, hid = pre_act.shape
        half = cotangent.shape[1]
        width = down_weight.shape[1]
        block = hid // reps
        if not (fs == 2 and tp == 1 and depth * CORES * ROWS == reps and depth == 4
                and block % 128 == 0 and half % 1024 == 0 and hid % 512 == 0 and tokens == 1024):
            return plain(pre_act, down_weight, cotangent)
        step = half // 4
        near = chunks_of(half, [step] * 4)
        far = chunks_of(half, [step] * 3 + [step // 2] * 2)
        nn, nf = len(near), len(far)
        total = nn + nf
        factor = 1.0 / float(tokens * reps) ** 0.5
        dma = lambda n: pltpu.SemaphoreType.DMA((n,))
        vm = pltpu.VMEM
        return pl.pallas_call(
            functools.partial(kernel, depth, near, far, step * 2, ORDER, factor),
            out_shape=[
                pltpu.VMEM((tokens, hid), BF16),
                pltpu.VMEM((block, width), F32),
            ],
            in_specs=[pl.BlockSpec(memory_space=pl.ANY)] * 3,
            out_specs=[pl.BlockSpec(memory_space=pltpu.VMEM)] * 2,
            scratch_shapes=[
                vm((tokens, hid), BF16),
                vm((2 * depth, tokens, block), BF16),
                vm((2 * depth * block, 2 * tokens), BF16),
                vm(down_weight.shape, BF16),
                vm((2, 2 * tokens, half), BF16),
                vm((tokens, hid), F32),
                vm((depth, block, width), BF16),
                vm((depth, block, width), BF16),
                vm((depth, block, width), F32),
                vm((depth, block, width), BF16),
                vm((depth, block, width), BF16),
                dma(4), dma(2 * depth), dma(2 * depth), dma(nn), dma(nn), dma(nf), dma(nf), dma(nf), dma(nf),
                dma(total), dma(total), dma(total * depth), dma(total * depth),
            ],
            compiler_params=pltpu.CompilerParams(
                collective_id=0, has_side_effects=True, vmem_limit_bytes=54 * 1024 * 1024
            ),
            cost_estimate=pl.CostEstimate(
                flops=8 * tokens * hid * width // 2, bytes_accessed=40 * 1024 * 1024, transcendentals=0),
        )(pre_act, down_weight, cotangent)

    return jax.shard_map(
        on_device,
        mesh=mesh,
        in_specs=(P("rep", ("fs", "tp")), P(("fs", "tp"), None), P("rep", ("fs", "tp"))),
        out_specs=(P("rep", ("fs", "tp")), P(("fs", "tp", "rep"), None)),
        check_vma=False,
    )
```

profile of v0, /device:TPU:0, one launch (start us, length us, event | category | flops | bytes accessed | tf_op | source)
XLA Modules:
  0.0 70.5 jit_solution(5555221362061521947)
XLA Ops:
  0.6 66.9 %shard_map.50 = (bf16[1024,2048]{1,0:T(8,128)(2,1)S(1)}, f32[128,2048]{1,0:T(8,128)S(1)}) custom-call(bf16[1024,2048]{1,0:T(8,128)(2,1)} %pre_hbm.1, bf16[2048,2048]{1,0:T(8,128)(2,1)} %w_hbm.1, bf16[1024,1024]{1,0:T(8,128)(2,1)} %cot_hbm.1), custom_call_target="tpu_custom_call" | custom-call | flops 17179869184 | bytes 41943040 | tf_op jit(solution)/shard_map/pallas_call | solution.py:359
  67.5 2.0 %copy.7 = bf16[1024,2048]{1,0:T(8,128)(2,1)} copy(bf16[1024,2048]{1,0:T(8,128)(2,1)S(1)} %get-tuple-element.2) | data formatting | bytes 8388608
  69.6 1.0 %copy.8 = f32[128,2048]{1,0:T(8,128)} copy(f32[128,2048]{1,0:T(8,128)S(1)} %get-tuple-element.3) | data formatting | bytes 2097152
where the time goes:
time: 70.7 us; the launch traced here: 70.5 us
  Pallas kernels  66.9 us (95%)
  local copies, waits for them, and re-layouts  2.99 us (4%)
    pallas_call x1, Pallas kernels, on_device(): pl.pallas_call(functools.partial(kernel, depth, near, far, step * 2, ORDE...  66.9 us
    unnamed x2, local copies, waits for them, and re-layouts  2.99 us

commit v1 on v0

v1 whole, which is shorter than its diff:
```python
import contextlib
import functools

import jax
import jax.numpy as jnp
from jax import lax
from jax.experimental import pallas as pl
from jax.experimental.pallas import tpu as pltpu
from jax.sharding import PartitionSpec as P

MESH = pl.DeviceIdType.MESH
CORES, ROWS = 2, 2
F32, BF16 = jnp.float32, jnp.bfloat16


NEAR, FAR = (4, 4, 4, 4), (4, 4, 2, 2, 2, 2)
CUTS = (2, 4)
FIRST_Z, RELAYS = 0, range(6)
ORDER = (
    "n0 n1 A1 o4",
    "n2 A0 n3 i4",
    "A3 g3 B0 g2",
    "B1 g1 x0 s1",
    "B3 f0 A4 t0",
    "B4 A2 B2 s3",
    "s4 x1 t3 f1",
    "t1 A5 t4 x2",
    "B5 h1 s2 f2",
    "h3 A6 v0 h2",
    "t2 x3 s5 f3",
    "A7 B7 l1 g0",
    "B6 l4 k3 s6",
    "x4 f4 A8 t5",
    "k2 l2 h0 x5",
    "f5 s7 l0 B8",
    "k0 x6 P9 f6",
    "A9 s8 k1 B9",
    "e2 e0 e1 s9.0",
    "e3 l6 l5 l3",
    "s9.1 s9.2 s9.3 l7",
    "l8 l9",
)


def scope(name):
    return contextlib.nullcontext()


def chunks_of(width, sizes):
    out, at = [], 0
    for s in sizes:
        out.append((at, s))
        at += s
    assert at == width
    return out


def plain(pre_act, down_weight, cotangent):
    whole = lax.all_gather(cotangent, ("fs", "tp"), axis=1, tiled=True)
    grad_hidden = lax.dot_general(
        whole, down_weight, (((1,), (1,)), ((), ())), preferred_element_type=F32
    )
    positive = jnp.maximum(pre_act.astype(F32), 0.0)
    grad_pre = (grad_hidden * 2.0 * positive).astype(BF16)
    hidden = (positive * positive).astype(BF16)
    factor = 1.0 / jnp.sqrt(jnp.float32(pre_act.shape[0] * lax.axis_size("rep")))
    term = lax.dot_general(
        hidden, whole, (((0,), (0,)), ((), ())), preferred_element_type=F32
    )
    summed = lax.psum_scatter(term, "rep", scatter_dimension=0, tiled=True)
    return (grad_pre, summed * factor)


def kernel(
    depth, near, far, crossing, marks, first_z, pieces, relays, order, factor,
    pre_hbm, w_hbm, cot_hbm, gp, gw,
    pre, pre_in, turned, w, cot, grad,
    y_out, y_in, own, z_out, z_in, b_sum, b_in, part,
    s_local, s_pre_s, s_pre_r, s_near_s, s_near_r, s_x_s, s_x_r, s_fwd_s, s_fwd_r,
    s_y_s, s_y_r, s_z_s, s_z_r, s_b_s, s_b_r,
):
    rep, fs, tp = lax.axis_index("rep"), lax.axis_index("fs"), lax.axis_index("tp")
    c, y, z = rep % CORES, (rep // CORES) % ROWS, rep // (CORES * ROWS)
    tokens, half = cot_hbm.shape
    hid = w_hbm.shape[0]
    block = own.shape[1]
    blocks = 2 * depth

    def at(z_, y_, c_, f_):
        return ((z_ * ROWS + y_) * CORES + c_, f_, tp)

    partner, across, beside = at(z, y, 1 - c, fs), at(z, y, c, 1 - fs), at(z, 1 - y, c, fs)

    def remote(src, dst, s, r, to):
        return pltpu.make_async_remote_copy(
            src_ref=src, dst_ref=dst, send_sem=s, recv_sem=r, device_id=to, device_id_type=MESH
        )

    def columns(i, c_):
        y_ = (1 - y) if i < depth else y
        k = (i % depth) * ROWS + y_
        return pl.ds(pl.multiple_of((k * CORES + c_) * block, block), block)

    def local(i, src, dst):
        return pltpu.make_async_copy(src, dst, s_local.at[i])

    loads = [local(0, pre_hbm, pre), local(1, cot_hbm, cot.at[0, pl.ds(0, tokens)]), local(2, w_hbm, w)]
    for l in loads:
        l.start()

    barrier = pltpu.get_barrier_semaphore()
    peers = [partner, across, beside]
    for d in range(1, depth):
        peers.append(at((z + d) % depth, y, c, fs))
    for p in peers:
        pl.semaphore_signal(barrier, inc=1, device_id=p, device_id_type=MESH)
    with scope("bar"):
        pl.semaphore_wait(barrier, len(peers))

    x_copies = []
    for q, (a, n, r, rn) in enumerate(crossing):
        x_copies.append(remote(
            cot_hbm.at[pl.ds(r, rn), pl.ds(a, n)], cot.at[1, pl.ds(r, rn), pl.ds(a, n)],
            s_x_s.at[q], s_x_r.at[q], across))
    x_copies[0].start()
    pre_copies = []
    for i in range(blocks):
        pre_copies.append(remote(
            pre_hbm.at[:, columns(i, 1 - c)], pre_in.at[i], s_pre_s.at[i], s_pre_r.at[i], partner))
    near_copies = []
    for q, (a, n) in enumerate(near):
        near_copies.append(remote(
            cot_hbm.at[:, pl.ds(a, n)], cot.at[0, pl.ds(tokens, tokens), pl.ds(a, n)],
            s_near_s.at[q], s_near_r.at[q], partner))
    for group in (pre_copies[:depth], near_copies[:2], pre_copies[depth:], near_copies[2:]):
        for copy in group:
            copy.start()
    for xc in x_copies[1:]:
        xc.start()

    def turn(v):
        p = jnp.maximum(v.astype(F32), 0.0)
        return (p * p).T.astype(BF16)

    strip = 256

    def turn_own(first):
        for i in range(first, first + depth):
            cols = columns(i, c)

            @pl.loop(0, tokens // strip, unroll=2)
            def _(t):
                rows = pl.ds(pl.multiple_of(t * strip, strip), strip)
                turned[pl.ds(i * block, block), rows] = turn(pre[rows, cols])

    def turn_in(first):
        for i in range(first, first + depth):
            pre_copies[i].wait_recv()

        @pl.loop(first, first + depth)
        def _(i):
            @pl.loop(0, tokens // strip, unroll=2)
            def _(t):
                rows = pl.ds(pl.multiple_of(t * strip, strip), strip)
                to = pl.ds(pl.multiple_of(tokens + t * strip, strip), strip)
                turned[pl.ds(pl.multiple_of(i * block, block), block), to] = turn(pre_in[i, rows, :])

    tall = 2 * block

    chunks = [(0, a, n) for a, n in near] + [(1, a, n) for a, n in far]

    def span(h, a, n):
        return pl.ds(h * half + a, n)

    def y_copy(j, p=0):
        h, a, n = chunks[j]
        s = span(h, a, n)
        if j == first_z:
            return remote(y_out.at[z, :, s], b_in, s_y_s.at[j], s_y_r.at[j], beside)
        each = depth // pieces[j]
        rows = pl.ds(p * each, each)
        return remote(
            y_out.at[rows, :, s], y_in.at[rows, :, s], s_y_s.at[j + p], s_y_r.at[j + p], beside)

    slots, far_end = depth, depth - 1
    inner = (z > 0) & (z < far_end)

    def relayed(j):
        return j in relays

    def z_block(j, kind):
        if kind == "up":
            ends = (z == far_end) if relayed(j) else False
            return jnp.where(ends, 0, (z + 1) % depth), jnp.where(ends, 3, 0), jnp.where(ends, far_end - 1, (z + 1) % depth)
        if kind == "down":
            ends = (z == 0) if relayed(j) else False
            return jnp.where(ends, far_end, (z + far_end) % depth), jnp.where(ends, 3, 2), jnp.where(ends, 1, (z + far_end) % depth)
        return (z + 2) % depth, 1, (z + 2) % depth

    def z_copy(j, kind, of_beside=False):
        h, a, n = chunks[j]
        s = span(h, a, n)
        block_, slot, to = z_block(j, kind)
        if of_beside:
            return remote(
                y_out.at[block_, :, s], y_in.at[slot, :, s], s_b_s.at[slot], s_b_r.at[slot], at(to, y, c, fs))
        return remote(
            z_out.at[block_, :, s], z_in.at[slot, :, s],
            s_z_s.at[j * slots + slot], s_z_r.at[j * slots + slot], at(to, y, c, fs))

    def z_arrival(j, slot, of_beside=False):
        h, a, n = chunks[j]
        s = span(h, a, n)
        if of_beside:
            return remote(y_out.at[0, :, s], y_in.at[slot, :, s], s_b_s.at[slot], s_b_r.at[slot], beside)
        return remote(
            z_out.at[0, :, s], z_in.at[slot, :, s],
            s_z_s.at[j * slots + slot], s_z_r.at[j * slots + slot], beside)

    def z_send(j, of_beside=False):
        z_copy(j, "up", of_beside).start()
        z_copy(j, "down", of_beside).start()
        if relayed(j):

            @pl.when(jnp.logical_not(inner))
            def _():
                z_copy(j, "two", of_beside).start()
        else:
            z_copy(j, "two", of_beside).start()

    def fwd_copy(q):
        a, n, r, rn = crossing[q]
        return remote(
            cot.at[1, pl.ds(r, rn), pl.ds(a, n)], cot.at[1, pl.ds(tokens + r, rn), pl.ds(a, n)],
            s_fwd_s.at[q], s_fwd_r.at[q], partner)

    def dot(j, m, which=None):
        h, a, n = chunks[j]
        rows = pl.ds(pl.multiple_of(m * tall, tall), tall)
        if which is None:
            return lax.dot_general(
                turned[rows, :], cot[h, :, pl.ds(a, n)], (((1,), (0,)), ((), ())),
                preferred_element_type=F32).reshape(2, block, n)
        r, rn = crossing[which][2:]

        def over(first):
            ts = pl.ds(first + r, rn)
            return lax.dot_general(
                turned[rows, ts], cot[h, ts, pl.ds(a, n)], (((1,), (0,)), ((), ())),
                preferred_element_type=F32)

        return (over(0) + over(tokens)).reshape(2, block, n)

    def product_start(j):
        h, a, n = chunks[j]
        s = span(h, a, n)
        for m in range(depth // 2):
            part[pl.ds(m * 2, 2)] = dot(j, m, -2)
            own[pl.ds(m * 2, 2), :, s] = dot(j, m + depth // 2, -2)

    def product_beside(j):
        h, a, n = chunks[j]
        s = span(h, a, n)
        if pieces[j] > 1:
            for m in range(depth // 2):
                y_out[pl.ds(m * 2, 2), :, s] = (part[pl.ds(m * 2, 2)] + dot(j, m, -1)).astype(BF16)
                y_copy(j, 2 * m).start()
                y_copy(j, 2 * m + 1).start()
            return

        @pl.loop(0, depth // 2, unroll=True)
        def _(m):
            y_out[pl.ds(m * 2, 2), :, s] = dot(j, m).astype(BF16)

        if j == first_z:
            b_sum[...] = y_out[z, :, s].astype(F32)
            z_send(j, True)
        else:
            y_copy(j).start()

    def product_own(j):
        h, a, n = chunks[j]
        s = span(h, a, n)
        if pieces[j] > 1:
            for m in range(depth // 2):
                own[pl.ds(m * 2, 2), :, s] += dot(j, m + depth // 2, -1)
            return

        @pl.loop(0, depth // 2, unroll=True)
        def _(m):
            v = dot(j, m + depth // 2)
            own[pl.ds(m * 2, 2), :, s] = v
            if j == first_z:
                z_out[pl.ds(m * 2, 2), :, s] = v.astype(BF16)

        if j == first_z:
            z_send(j)

    def second(j, p=0):
        h, a, n = chunks[j]
        s = span(h, a, n)
        each = depth // pieces[j]
        with scope(f"wy{j}"):
            y_copy(j, p).wait_recv()

        @pl.loop(p * each, (p + 1) * each, unroll=each < depth)
        def _(k):
            v = own[k, :, s] + y_in[k, :, s].astype(F32)
            own[k, :, s] = v
            z_out[k, :, s] = v.astype(BF16)

        if pieces[j] == 1:
            z_send(j)
            return
        for kind in ("up", "down", "two"):

            @pl.when(z_block(j, kind)[0] // each == p)
            def _(kind=kind):
                z_copy(j, kind).start()

    def third(j):
        h, a, n = chunks[j]
        s = span(h, a, n)

        @pl.when(inner)
        def _():
            to = (z + 2) % depth
            with scope(f"wr{j}"):
                z_arrival(j, 3).wait_recv()
            z_out[to, :, s] = (own[to, :, s] + z_in[3, :, s].astype(F32)).astype(BF16)
            z_copy(j, "two").start()
            if j == first_z:
                z_arrival(j, 3, True).wait_recv()
                y_out[to, :, s] = (y_out[to, :, s].astype(F32) + y_in[3, :, s].astype(F32)).astype(BF16)
                z_copy(j, "two", True).start()

    def arrivals(j, add):
        for slot, there in ((0, z > 0), (2, z < far_end), (1, None)) if relayed(j) else ((0, None), (2, None), (1, None)):
            if there is None:
                add(slot)
            else:
                pl.when(there)(functools.partial(add, slot))

    def across_z(j):
        h, a, n = chunks[j]
        s = span(h, a, n)

        def add(slot):
            with scope(f"wb{j}s{slot}"):
                z_arrival(j, slot, True).wait_recv()
            b_sum[...] += y_in[slot, :, s].astype(F32)

        arrivals(j, add)
        y_out[z, :, s] = b_sum[...].astype(BF16)
        y_copy(j).start()

    def last(j):
        h, a, n = chunks[j]
        s = span(h, a, n)

        def add(slot):
            with scope(f"wz{j}s{slot}"):
                z_arrival(j, slot).wait_recv()
            own[z, :, s] = own[z, :, s] + z_in[slot, :, s].astype(F32)

        arrivals(j, add)
        place = pl.multiple_of((fs if h == 0 else 1 - fs) * half + a, 128)
        total_ = own[z, :, s]
        if j == first_z:
            y_copy(j).wait_recv()
            total_ = total_ + b_in[...].astype(F32)
        gw[:, pl.ds(place, n)] = total_ * factor

    tm, tn = 256, 512

    def grad_tile(h, a, n, m, k):
        rows = pl.ds(pl.multiple_of(m * tm, tm), tm)
        outs = pl.ds(pl.multiple_of(k * tn, tn), tn)
        place = pl.multiple_of((fs if h == 0 else 1 - fs) * half + a, 128)
        return rows, outs, lax.dot_general(
            cot[h, rows, pl.ds(a, n)], w[outs, pl.ds(place, n)], (((1,), (1,)), ((), ())),
            preferred_element_type=F32)

    weights = [loads[2]]

    def grad_first(m):
        if weights:
            weights.pop().wait()

        @pl.loop(0, hid // tn, unroll=True)
        def _(k):
            rows, outs, v = grad_tile(0, 0, half, m, k)
            grad[rows, outs] = v

    def grad_next(m, part):
        @pl.loop(0, hid // tn, unroll=True)
        def _(k):
            rows, outs, v = grad_tile(1, marks[part], marks[part + 1] - marks[part], m, k)
            grad[rows, outs] += v

    def grad_rest(m):
        @pl.loop(0, hid // tn, unroll=True)
        def _(k):
            rows, outs, v = grad_tile(1, marks[-2], marks[-1] - marks[-2], m, k)
            p = jnp.maximum(pre[rows, outs].astype(F32), 0.0)
            gp[rows, outs] = ((grad[rows, outs] + v) * 2.0 * p).astype(BF16)

    def near_in(q):
        near_copies[q].wait_recv()

    def far_in(q):
        x_copies[q].wait_recv()
        fwd_copy(q).start()

    def far_both(q):
        fwd_copy(q).wait_recv()

    nn, nf = len(near), len(far)
    total = nn + nf
    steps = {
        "A": product_beside, "B": product_own, "P": product_start,
        "s": second, "t": third, "v": across_z, "l": last, "n": near_in, "x": far_in, "f": far_both,
        "g": grad_first, "h": lambda m: grad_next(m, 0), "k": lambda m: grad_next(m, 1), "e": grad_rest,
        "o": turn_own, "i": turn_in,
    }
    with scope("ld0"):
        loads[0].wait()
    with scope("o0"):
        turn_own(0)
    loads[1].wait()
    with scope("i0"):
        turn_in(0)
    for step in " ".join(order).split():
        with scope(step):
            steps[step[0]](*(int(v) for v in step[1:].split(".")))

    with scope("drain"):
        for copy in pre_copies + near_copies + x_copies:
            copy.wait_send()
        for q in range(len(crossing)):
            fwd_copy(q).wait_send()
        for j in range(total):
            for p in range(pieces[j]):
                y_copy(j, p).wait_send()
            for kind in ("up", "down", "two"):
                z_copy(j, kind).wait_send()
                if j == first_z:
                    z_copy(j, kind, True).wait_send()


def solution(mesh):
    reps, fs, tp = mesh.shape["rep"], mesh.shape["fs"], mesh.shape["tp"]
    depth = reps // (CORES * ROWS)

    def on_device(pre_act, down_weight, cotangent):
        tokens, hid = pre_act.shape
        half = cotangent.shape[1]
        width = down_weight.shape[1]
        block = hid // reps
        if not (fs == 2 and tp == 1 and depth * CORES * ROWS == reps and depth == 4
                and block % 128 == 0 and half % 1024 == 0 and hid % 512 == 0 and tokens == 1024):
            return plain(pre_act, down_weight, cotangent)
        step = half // 4
        near = chunks_of(half, [step // 4 * v for v in NEAR])
        far = chunks_of(half, [step // 4 * v for v in FAR])
        nn, nf = len(near), len(far)
        total = nn + nf
        marks = [0] + [far[i][0] for i in CUTS] + [half]
        crossing = [(a, n, 0, tokens) for a, n in far]
        a, n = far[-1]
        crossing[-1:] = [(a, n, 0, tokens // 2), (a, n, tokens // 2, tokens // 2)]
        nx = len(crossing)
        pieces = [1] * (total - 1) + [depth]
        first_z, relays = FIRST_Z, RELAYS
        factor = 1.0 / float(tokens * reps) ** 0.5
        dma = lambda n: pltpu.SemaphoreType.DMA((n,))
        vm = pltpu.VMEM
        return pl.pallas_call(
            functools.partial(kernel, depth, near, far, crossing, marks, first_z, pieces, relays, ORDER, factor),
            out_shape=[
                pltpu.VMEM((tokens, hid), BF16),
                pltpu.VMEM((block, width), F32),
            ],
            in_specs=[pl.BlockSpec(memory_space=pl.ANY)] * 3,
            out_specs=[pl.BlockSpec(memory_space=pltpu.VMEM)] * 2,
            scratch_shapes=[
                vm((tokens, hid), BF16),
                vm((2 * depth, tokens, block), BF16),
                vm((2 * depth * block, 2 * tokens), BF16),
                vm(down_weight.shape, BF16),
                vm((2, 2 * tokens, half), BF16),
                vm((tokens, hid), F32),
                vm((depth, block, width), BF16),
                vm((depth, block, width), BF16),
                vm((depth, block, width), F32),
                vm((depth, block, width), BF16),
                vm((depth, block, width), BF16),
                vm((block, near[0][1]), F32),
                vm((block, near[0][1]), BF16),
                vm((depth, block, far[-1][1]), F32),
                dma(4), dma(2 * depth), dma(2 * depth), dma(nn), dma(nn), dma(nx), dma(nx), dma(nx), dma(nx),
                dma(total + depth), dma(total + depth), dma(total * depth), dma(total * depth), dma(depth), dma(depth),
            ],
            compiler_params=pltpu.CompilerParams(
                collective_id=0, has_side_effects=True, vmem_limit_bytes=56 * 1024 * 1024
            ),
            cost_estimate=pl.CostEstimate(
                flops=8 * tokens * hid * width // 2, bytes_accessed=40 * 1024 * 1024, transcendentals=0),
        )(pre_act, down_weight, cotangent)

    return jax.shard_map(
        on_device,
        mesh=mesh,
        in_specs=(P("rep", ("fs", "tp")), P(("fs", "tp"), None), P("rep", ("fs", "tp"))),
        out_specs=(P("rep", ("fs", "tp")), P(("fs", "tp", "rep"), None)),
        check_vma=False,
    )
```

time: 70.7 us -> 67.6 us (0.956)
  Pallas kernels: 66.9 us -> 63.8 us
    pallas_call x1, Pallas kernels: 66.9 us -> 63.8 us  [on_device(): pl.pallas_call(functools.partial(kernel, depth, near, far, crossing, mark...]
where the time goes in v1:
time: 67.6 us; the launch traced here: 67.4 us
  Pallas kernels  63.8 us (94%)
  local copies, waits for them, and re-layouts  2.99 us (4%)
    pallas_call x1, Pallas kernels, on_device(): pl.pallas_call(functools.partial(kernel, depth, near, far, crossing, mark...  63.8 us
    unnamed x2, local copies, waits for them, and re-layouts  2.99 us

profile of v1, /device:TPU:0, one launch (start us, length us, event | category | flops | bytes accessed | tf_op | source)
XLA Modules:
  0.0 67.4 jit_solution(12702093377188252019)
XLA Ops:
  0.6 63.8 %shard_map.50 = (bf16[1024,2048]{1,0:T(8,128)(2,1)S(1)}, f32[128,2048]{1,0:T(8,128)S(1)}) custom-call(bf16[1024,2048]{1,0:T(8,128)(2,1)} %pre_hbm.1, bf16[2048,2048]{1,0:T(8,128)(2,1)} %w_hbm.1, bf16[1024,1024]{1,0:T(8,128)(2,1)} %cot_hbm.1), custom_call_target="tpu_custom_call" | custom-call | flops 17179869184 | bytes 41943040 | tf_op jit(solution)/shard_map/pallas_call | solution.py:478
  64.5 2.0 %copy.7 = bf16[1024,2048]{1,0:T(8,128)(2,1)} copy(bf16[1024,2048]{1,0:T(8,128)(2,1)S(1)} %get-tuple-element.2) | data formatting | bytes 8388608
  66.5 1.0 %copy.8 = f32[128,2048]{1,0:T(8,128)} copy(f32[128,2048]{1,0:T(8,128)S(1)} %get-tuple-element.3) | data formatting | bytes 2097152

commit v2 on v1

--- a/solution.py
+++ b/solution.py
@@ -17,28 +17,27 @@
 CUTS = (2, 4)
 FIRST_Z, RELAYS = 0, range(6)
 ORDER = (
-    "n0 n1 A1 o4",
-    "n2 A0 n3 i4",
-    "A3 g3 B0 g2",
-    "B1 g1 x0 s1",
-    "B3 f0 A4 t0",
-    "B4 A2 B2 s3",
-    "s4 x1 t3 f1",
-    "t1 A5 t4 x2",
-    "B5 h1 s2 f2",
-    "h3 A6 v0 h2",
-    "t2 x3 s5 f3",
-    "A7 B7 l1 g0",
-    "B6 l4 k3 s6",
-    "x4 f4 A8 t5",
-    "k2 l2 h0 x5",
-    "f5 s7 l0 B8",
-    "k0 x6 P9 f6",
-    "A9 s8 k1 B9",
-    "e2 e0 e1 s9.0",
-    "e3 l6 l5 l3",
-    "s9.1 s9.2 s9.3 l7",
-    "l8 l9",
+    "n0 o4 n1 A1",
+    "i4 n2 A0 n3",
+    "A3 B3 B1 B0",
+    "g3 g0 x0 s1",
+    "g2 f0 A4 A2",
+    "B2 s3 t0 B4",
+    "t3 g1 x1 s4",
+    "t1 f1 A5 B5",
+    "h0 h1 h2 h3",
+    "s2 t4 x2 v0",
+    "f2 A6 B6 s5",
+    "t2 x3 f3 A7",
+    "B7 k0 k1 t5",
+    "s6 k2 k3 x4",
+    "f4 A8 B8 x5",
+    "s7 x6 f5 P9",
+    "f6 A9 s8.0 B9",
+    "s8.1 e0 s8.2 s8.3",
+    "e1 s9.0 l6 s9.1",
+    "s9.2 l7 s9.3 e2",
+    "e3 L0 l8 l9",
 )
 
 
@@ -76,8 +75,7 @@
     pre_hbm, w_hbm, cot_hbm, gp, gw,
     pre, pre_in, turned, w, cot, grad,
     y_out, y_in, own, z_out, z_in, b_sum, b_in, part,
-    s_local, s_pre_s, s_pre_r, s_near_s, s_near_r, s_x_s, s_x_r, s_fwd_s, s_fwd_r,
-    s_y_s, s_y_r, s_z_s, s_z_r, s_b_s, s_b_r,
+    s_above, s_local, s_sent, s_pre_r, s_near_r, s_x_r, s_fwd_r, s_y_r, s_z_r, s_b_r,
 ):
     rep, fs, tp = lax.axis_index("rep"), lax.axis_index("fs"), lax.axis_index("tp")
     c, y, z = rep % CORES, (rep // CORES) % ROWS, rep // (CORES * ROWS)
@@ -104,40 +102,49 @@
     def local(i, src, dst):
         return pltpu.make_async_copy(src, dst, s_local.at[i])
 
-    loads = [local(0, pre_hbm, pre), local(1, cot_hbm, cot.at[0, pl.ds(0, tokens)]), local(2, w_hbm, w)]
+    loads = [local(0, cot_hbm, cot.at[0, pl.ds(0, tokens)]), local(1, pre_hbm, pre), local(2, w_hbm, w)]
     for l in loads:
         l.start()
 
     barrier = pltpu.get_barrier_semaphore()
-    peers = [partner, across, beside]
+    for p in (partner, across, beside):
+        pl.semaphore_signal(barrier, inc=1, device_id=p, device_id_type=MESH)
     for d in range(1, depth):
-        peers.append(at((z + d) % depth, y, c, fs))
-    for p in peers:
-        pl.semaphore_signal(barrier, inc=1, device_id=p, device_id_type=MESH)
+
+        @pl.when(z + d < depth)
+        def _(d=d):
+            pl.semaphore_signal(barrier, inc=1, device_id=at(z + d, y, c, fs), device_id_type=MESH)
+
     with scope("bar"):
-        pl.semaphore_wait(barrier, len(peers))
+        pl.semaphore_wait(barrier, 3 + z)
+    for d in range(1, depth):
+
+        @pl.when(z >= d)
+        def _(d=d):
+            pl.semaphore_signal(s_above, inc=1, device_id=at(z - d, y, c, fs), device_id_type=MESH)
 
     x_copies = []
     for q, (a, n, r, rn) in enumerate(crossing):
         x_copies.append(remote(
-            cot_hbm.at[pl.ds(r, rn), pl.ds(a, n)], cot.at[1, pl.ds(r, rn), pl.ds(a, n)],
-            s_x_s.at[q], s_x_r.at[q], across))
-    x_copies[0].start()
+            cot.at[0, pl.ds(r, rn), pl.ds(a, n)], cot.at[1, pl.ds(r, rn), pl.ds(a, n)],
+            s_sent.at[2], s_x_r.at[q], across))
     pre_copies = []
     for i in range(blocks):
         pre_copies.append(remote(
-            pre_hbm.at[:, columns(i, 1 - c)], pre_in.at[i], s_pre_s.at[i], s_pre_r.at[i], partner))
+            pre.at[:, columns(i, 1 - c)], pre_in.at[i], s_sent.at[0], s_pre_r.at[i // depth], partner))
     near_copies = []
     for q, (a, n) in enumerate(near):
         near_copies.append(remote(
-            cot_hbm.at[:, pl.ds(a, n)], cot.at[0, pl.ds(tokens, tokens), pl.ds(a, n)],
-            s_near_s.at[q], s_near_r.at[q], partner))
+            cot.at[0, pl.ds(0, tokens), pl.ds(a, n)], cot.at[0, pl.ds(tokens, tokens), pl.ds(a, n)],
+            s_sent.at[1], s_near_r.at[q], partner))
+    with scope("ld"):
+        loads[0].wait()
+    for xc in x_copies:
+        xc.start()
+    loads[1].wait()
     for group in (pre_copies[:depth], near_copies[:2], pre_copies[depth:], near_copies[2:]):
         for copy in group:
             copy.start()
-    for xc in x_copies[1:]:
-        xc.start()
-
     def turn(v):
         p = jnp.maximum(v.astype(F32), 0.0)
         return (p * p).T.astype(BF16)
@@ -154,8 +161,8 @@
                 turned[pl.ds(i * block, block), rows] = turn(pre[rows, cols])
 
     def turn_in(first):
-        for i in range(first, first + depth):
-            pre_copies[i].wait_recv()
+        both = pre_in.at[pl.ds(first, depth)]
+        remote(both, both, s_sent.at[0], s_pre_r.at[first // depth], partner).wait_recv()
 
         @pl.loop(first, first + depth)
         def _(i):
@@ -169,18 +176,22 @@
 
     chunks = [(0, a, n) for a, n in near] + [(1, a, n) for a, n in far]
 
+    final = len(chunks) - 1
+
     def span(h, a, n):
         return pl.ds(h * half + a, n)
 
+    def turn_of(p):
+        return jnp.where(c == 0, p, p + 1 - 2 * (p % 2))
+
     def y_copy(j, p=0):
         h, a, n = chunks[j]
         s = span(h, a, n)
         if j == first_z:
-            return remote(y_out.at[z, :, s], b_in, s_y_s.at[j], s_y_r.at[j], beside)
-        each = depth // pieces[j]
-        rows = pl.ds(p * each, each)
+            return remote(y_out.at[z, :, s], b_in, s_sent.at[5], s_y_r.at[sum(pieces[:j])], beside)
+        rows = pl.ds(turn_of(p), 1) if pieces[j] > 1 else pl.ds(0, depth)
         return remote(
-            y_out.at[rows, :, s], y_in.at[rows, :, s], s_y_s.at[j + p], s_y_r.at[j + p], beside)
+            y_out.at[rows, :, s], y_in.at[rows, :, s], s_sent.at[4], s_y_r.at[sum(pieces[:j]) + p], beside)
 
     slots, far_end = depth, depth - 1
     inner = (z > 0) & (z < far_end)
@@ -201,21 +212,20 @@
         h, a, n = chunks[j]
         s = span(h, a, n)
         block_, slot, to = z_block(j, kind)
+        relay = jnp.where(slot == 3, 1, 0)
         if of_beside:
             return remote(
-                y_out.at[block_, :, s], y_in.at[slot, :, s], s_b_s.at[slot], s_b_r.at[slot], at(to, y, c, fs))
+                y_out.at[block_, :, s], y_in.at[slot, :, s], s_sent.at[7], s_b_r.at[relay], at(to, y, c, fs))
         return remote(
             z_out.at[block_, :, s], z_in.at[slot, :, s],
-            s_z_s.at[j * slots + slot], s_z_r.at[j * slots + slot], at(to, y, c, fs))
-
-    def z_arrival(j, slot, of_beside=False):
-        h, a, n = chunks[j]
-        s = span(h, a, n)
-        if of_beside:
-            return remote(y_out.at[0, :, s], y_in.at[slot, :, s], s_b_s.at[slot], s_b_r.at[slot], beside)
-        return remote(
-            z_out.at[0, :, s], z_in.at[slot, :, s],
-            s_z_s.at[j * slots + slot], s_z_r.at[j * slots + slot], beside)
+            s_sent.at[6], s_z_r.at[relay * (1 + j) if relayed(j) else 1 + j], at(to, y, c, fs))
+
+    def arrived(ref, sem):
+        remote(ref, ref, s_sent.at[6], sem, beside).wait_recv()
+
+    def all_arrived(ref, cols, sem):
+        pl.when(inner)(lambda: arrived(ref.at[pl.ds(0, 3), :, cols], sem))
+        pl.when(jnp.logical_not(inner))(lambda: arrived(ref.at[pl.ds(0, 2), :, cols], sem))
 
     def z_send(j, of_beside=False):
         z_copy(j, "up", of_beside).start()
@@ -232,7 +242,7 @@
         a, n, r, rn = crossing[q]
         return remote(
             cot.at[1, pl.ds(r, rn), pl.ds(a, n)], cot.at[1, pl.ds(tokens + r, rn), pl.ds(a, n)],
-            s_fwd_s.at[q], s_fwd_r.at[q], partner)
+            s_sent.at[3], s_fwd_r.at[q], partner)
 
     def dot(j, m, which=None):
         h, a, n = chunks[j]
@@ -263,7 +273,8 @@
         s = span(h, a, n)
         if pieces[j] > 1:
             for m in range(depth // 2):
-                y_out[pl.ds(m * 2, 2), :, s] = (part[pl.ds(m * 2, 2)] + dot(j, m, -1)).astype(BF16)
+                v = part[pl.ds(m * 2, 2)] + dot(j, m, -1) if j == final else dot(j, m)
+                y_out[pl.ds(m * 2, 2), :, s] = v.astype(BF16)
                 y_copy(j, 2 * m).start()
                 y_copy(j, 2 * m + 1).start()
             return
@@ -281,7 +292,7 @@
     def product_own(j):
         h, a, n = chunks[j]
         s = span(h, a, n)
-        if pieces[j] > 1:
+        if j == final:
             for m in range(depth // 2):
                 own[pl.ds(m * 2, 2), :, s] += dot(j, m + depth // 2, -1)
             return
@@ -299,22 +310,23 @@
     def second(j, p=0):
         h, a, n = chunks[j]
         s = span(h, a, n)
-        each = depth // pieces[j]
         with scope(f"wy{j}"):
             y_copy(j, p).wait_recv()
 
-        @pl.loop(p * each, (p + 1) * each, unroll=each < depth)
-        def _(k):
+        def add(k):
             v = own[k, :, s] + y_in[k, :, s].astype(F32)
             own[k, :, s] = v
             z_out[k, :, s] = v.astype(BF16)
 
         if pieces[j] == 1:
+            pl.loop(0, depth)(add)
             z_send(j)
             return
+        k = turn_of(p)
+        add(k)
         for kind in ("up", "down", "two"):
 
-            @pl.when(z_block(j, kind)[0] // each == p)
+            @pl.when(z_block(j, kind)[0] == k)
             def _(kind=kind):
                 z_copy(j, kind).start()
 
@@ -326,11 +338,11 @@
         def _():
             to = (z + 2) % depth
             with scope(f"wr{j}"):
-                z_arrival(j, 3).wait_recv()
+                arrived(z_in.at[3, :, s], s_z_r.at[1 + j])
             z_out[to, :, s] = (own[to, :, s] + z_in[3, :, s].astype(F32)).astype(BF16)
             z_copy(j, "two").start()
             if j == first_z:
-                z_arrival(j, 3, True).wait_recv()
+                arrived(y_in.at[3, :, s], s_b_r.at[1])
                 y_out[to, :, s] = (y_out[to, :, s].astype(F32) + y_in[3, :, s].astype(F32)).astype(BF16)
                 z_copy(j, "two", True).start()
 
@@ -344,32 +356,45 @@
     def across_z(j):
         h, a, n = chunks[j]
         s = span(h, a, n)
+        with scope("wb"):
+            all_arrived(y_in, s, s_b_r.at[0])
 
         def add(slot):
-            with scope(f"wb{j}s{slot}"):
-                z_arrival(j, slot, True).wait_recv()
             b_sum[...] += y_in[slot, :, s].astype(F32)
 
         arrivals(j, add)
         y_out[z, :, s] = b_sum[...].astype(BF16)
         y_copy(j).start()
 
-    def last(j):
+    def total_of(j):
         h, a, n = chunks[j]
         s = span(h, a, n)
 
         def add(slot):
-            with scope(f"wz{j}s{slot}"):
-                z_arrival(j, slot).wait_recv()
             own[z, :, s] = own[z, :, s] + z_in[slot, :, s].astype(F32)
 
         arrivals(j, add)
         place = pl.multiple_of((fs if h == 0 else 1 - fs) * half + a, 128)
-        total_ = own[z, :, s]
+        v = own[z, :, s]
         if j == first_z:
-            y_copy(j).wait_recv()
-            total_ = total_ + b_in[...].astype(F32)
-        gw[:, pl.ds(place, n)] = total_ * factor
+            v = v + b_in[...].astype(F32)
+        gw[:, pl.ds(place, n)] = v * factor
+
+    def last(j):
+        h, a, n = chunks[j]
+        with scope(f"wz{j}"):
+            arrived(z_in.at[pl.ds(0, 3), :, span(h, a, n)], s_z_r.at[1 + j])
+        total_of(j)
+
+    def last_relayed(_):
+        h, a, n = chunks[len(relays) - 1]
+        with scope("wL"):
+            all_arrived(z_in, pl.ds(0, h * half + a + n), s_z_r.at[0])
+        with scope("wLy"):
+            if first_z is not None:
+                y_copy(first_z).wait_recv()
+        for j in relays:
+            total_of(j)
 
     tm, tn = 256, 512
 
@@ -419,33 +444,47 @@
     total = nn + nf
     steps = {
         "A": product_beside, "B": product_own, "P": product_start,
-        "s": second, "t": third, "v": across_z, "l": last, "n": near_in, "x": far_in, "f": far_both,
+        "s": second, "t": third, "v": across_z, "l": last, "L": last_relayed, "n": near_in, "x": far_in, "f": far_both,
         "g": grad_first, "h": lambda m: grad_next(m, 0), "k": lambda m: grad_next(m, 1), "e": grad_rest,
         "o": turn_own, "i": turn_in,
     }
-    with scope("ld0"):
-        loads[0].wait()
     with scope("o0"):
         turn_own(0)
-    loads[1].wait()
     with scope("i0"):
         turn_in(0)
+    with scope("above"):
+        pl.when(z < depth - 1)(lambda: pl.semaphore_wait(s_above, depth - 1 - z))
     for step in " ".join(order).split():
         with scope(step):
             steps[step[0]](*(int(v) for v in step[1:].split(".")))
 
     with scope("drain"):
-        for copy in pre_copies + near_copies + x_copies:
-            copy.wait_send()
-        for q in range(len(crossing)):
-            fwd_copy(q).wait_send()
-        for j in range(total):
-            for p in range(pieces[j]):
-                y_copy(j, p).wait_send()
-            for kind in ("up", "down", "two"):
-                z_copy(j, kind).wait_send()
-                if j == first_z:
-                    z_copy(j, kind, True).wait_send()
+        skip = 0 if first_z is None else near[0][1]
+        whole = cot.at[0, pl.ds(0, tokens)]
+        first = pl.ds(0, skip)
+        sent = [
+            pre.at[:, pl.ds(0, blocks * block)], whole, whole, whole,
+            y_out.at[:, :, pl.ds(skip, 2 * half - skip)], y_out.at[0, :, first],
+            z_out.at[pl.ds(0, 3)], y_out.at[pl.ds(0, 3), :, first],
+        ]
+        for i, ref in enumerate(sent):
+            if skip or i not in (5, 7):
+                remote(ref, ref, s_sent.at[i], s_b_r.at[0], partner).wait_send()
+
+
+PARTS = 4
+
+
+def store(gp_in, gw_in, gp_out, gw_out, sems):
+    rows = gp_in.shape[0] // PARTS
+    copies = [pltpu.make_async_copy(gw_in, gw_out, sems.at[PARTS])]
+    for i in range(PARTS):
+        r = pl.ds(i * rows, rows)
+        copies.append(pltpu.make_async_copy(gp_in.at[r], gp_out.at[r], sems.at[i]))
+    for copy in copies:
+        copy.start()
+    for copy in copies:
+        copy.wait()
 
 
 def solution(mesh):
@@ -470,12 +509,12 @@
         a, n = far[-1]
         crossing[-1:] = [(a, n, 0, tokens // 2), (a, n, tokens // 2, tokens // 2)]
         nx = len(crossing)
-        pieces = [1] * (total - 1) + [depth]
+        pieces = [1] * (total - 2) + [depth] * 2
         first_z, relays = FIRST_Z, RELAYS
         factor = 1.0 / float(tokens * reps) ** 0.5
         dma = lambda n: pltpu.SemaphoreType.DMA((n,))
         vm = pltpu.VMEM
-        return pl.pallas_call(
+        results = pl.pallas_call(
             functools.partial(kernel, depth, near, far, crossing, marks, first_z, pieces, relays, ORDER, factor),
             out_shape=[
                 pltpu.VMEM((tokens, hid), BF16),
@@ -498,8 +537,8 @@
                 vm((block, near[0][1]), F32),
                 vm((block, near[0][1]), BF16),
                 vm((depth, block, far[-1][1]), F32),
-                dma(4), dma(2 * depth), dma(2 * depth), dma(nn), dma(nn), dma(nx), dma(nx), dma(nx), dma(nx),
-                dma(total + depth), dma(total + depth), dma(total * depth), dma(total * depth), dma(depth), dma(depth),
+                pltpu.SemaphoreType.REGULAR, dma(3), dma(8), dma(2), dma(nn), dma(nx), dma(nx),
+                dma(sum(pieces)), dma(1 + total), dma(2),
             ],
             compiler_params=pltpu.CompilerParams(
                 collective_id=0, has_side_effects=True, vmem_limit_bytes=56 * 1024 * 1024
@@ -507,6 +546,18 @@
             cost_estimate=pl.CostEstimate(
                 flops=8 * tokens * hid * width // 2, bytes_accessed=40 * 1024 * 1024, transcendentals=0),
         )(pre_act, down_weight, cotangent)
+        return pl.pallas_call(
+            store,
+            out_shape=[
+                jax.ShapeDtypeStruct((tokens, hid), BF16),
+                jax.ShapeDtypeStruct((block, width), F32),
+            ],
+            in_specs=[pl.BlockSpec(memory_space=pl.ANY)] * 2,
+            out_specs=[pl.BlockSpec(memory_space=pl.ANY)] * 2,
+            scratch_shapes=[dma(PARTS + 1)],
+            compiler_params=pltpu.CompilerParams(vmem_limit_bytes=1024 * 1024),
+            cost_estimate=pl.CostEstimate(flops=1, bytes_accessed=10 * 1024 * 1024, transcendentals=0),
+        )(*results)
 
     return jax.shard_map(
         on_device,

time: 67.6 us -> 65.2 us (0.964)
  local copies, waits for them, and re-layouts: 2.99 us -> 0 us
    unnamed x2 -> x0, local copies, waits for them, and re-layouts: 2.99 us -> none
    pallas_call x0 -> x1, Pallas kernels: none -> 2.4 us  [on_device(): pl.pallas_call(store, out_shape=[jax.ShapeDtypeStruct((tokens, hid), BF16...]
    pallas_call x1, Pallas kernels: 63.8 us -> 61.9 us  [on_device(): pl.pallas_call(functools.partial(kernel, depth, near, far, crossing, mark...]
where the time goes in v2:
time: 65.2 us; the launch traced here: 65.1 us
  Pallas kernels  64.3 us (99%)
  between operations  0.82 us (1%)
    pallas_call x1, Pallas kernels, on_device(): pl.pallas_call(functools.partial(kernel, depth, near, far, crossing, mark...  61.9 us
    pallas_call x1, Pallas kernels, on_device(): pl.pallas_call(store, out_shape=[jax.ShapeDtypeStruct((tokens, hid), BF16...  2.4 us

profile of v2, /device:TPU:0, one launch (start us, length us, event | category | flops | bytes accessed | tf_op | source)
XLA Modules:
  0.0 65.1 jit_solution(8005072085759372428)
XLA Ops:
  0.6 61.9 %shard_map.50 = (bf16[1024,2048]{1,0:T(8,128)(2,1)S(1)}, f32[128,2048]{1,0:T(8,128)S(1)}) custom-call(bf16[1024,2048]{1,0:T(8,128)(2,1)} %pre_hbm.1, bf16[2048,2048]{1,0:T(8,128)(2,1)} %w_hbm.1, bf16[1024,1024]{1,0:T(8,128)(2,1)} %cot_hbm.1), custom_call_target="tpu_custom_call" | custom-call | flops 17179869184 | bytes 41943040 | tf_op jit(solution)/shard_map/pallas_call | solution.py:517
  62.5 2.4 %shard_map.51 = (bf16[1024,2048]{1,0:T(8,128)(2,1)}, f32[128,2048]{1,0:T(8,128)}) custom-call(bf16[1024,2048]{1,0:T(8,128)(2,1)S(1)} %get-tuple-element.4.gp_in, f32[128,2048]{1,0:T(8,128)S(1)} %get-tuple-element.5.gw_in), custom_call_target="tpu_custom_call" | custom-call | flops 1 | bytes 10485760 | tf_op jit(solution)/shard_map/pallas_call | solution.py:549

commit v3 on v2

--- a/solution.py
+++ b/solution.py
@@ -15,28 +15,28 @@
 
 NEAR, FAR = (4, 4, 4, 4), (4, 4, 2, 2, 2, 2)
 CUTS = (2, 4)
-FIRST_Z, RELAYS = 0, range(6)
+FIRST_Z, RELAYS = 0, range(8)
 ORDER = (
-    "n0 o4 n1 A1",
-    "i4 n2 A0 n3",
-    "A3 B3 B1 B0",
-    "g3 g0 x0 s1",
-    "g2 f0 A4 A2",
-    "B2 s3 t0 B4",
-    "t3 g1 x1 s4",
-    "t1 f1 A5 B5",
-    "h0 h1 h2 h3",
-    "s2 t4 x2 v0",
-    "f2 A6 B6 s5",
-    "t2 x3 f3 A7",
-    "B7 k0 k1 t5",
-    "s6 k2 k3 x4",
+    "n0 A0 n1 A1",
+    "o4 i4 B0 n2",
+    "A2 n3 A3 B1",
+    "g3 g0 x0 B2",
+    "s1 f0 A4 B3",
+    "t0 B4 g1 g2",
+    "s2 t1 x1 f1",
+    "A5 B5 v0 s3",
+    "h0 h1 t2 h2",
+    "h3 x2 s4 f2",
+    "A6 B6 t3 x3",
+    "s5 f3 A7 B7",
+    "k0 t4 s6 k1",
+    "k2 x4 t5 k3",
     "f4 A8 B8 x5",
-    "s7 x6 f5 P9",
-    "f6 A9 s8.0 B9",
-    "s8.1 e0 s8.2 s8.3",
-    "e1 s9.0 l6 s9.1",
-    "s9.2 l7 s9.3 e2",
+    "s7 t6 s8.0 x6",
+    "f5 s8.1 P9 f6",
+    "A9 t7 s8.2 s8.3",
+    "B9 e0 e1 s9.0",
+    "s9.1 s9.2 s9.3 e2",
     "e3 L0 l8 l9",
 )
 

time: 65.2 us -> 64.8 us (level)
  no operation moved by 1% of the time
where the time goes in v3:
time: 64.8 us; the launch traced here: 64.7 us
  Pallas kernels  63.9 us (99%)
  between operations  0.8 us (1%)
    pallas_call x1, Pallas kernels, on_device(): pl.pallas_call(functools.partial(kernel, depth, near, far, crossing, mark...  61.5 us
    pallas_call x1, Pallas kernels, on_device(): pl.pallas_call(store, out_shape=[jax.ShapeDtypeStruct((tokens, hid), BF16...  2.4 us

profile of v3, /device:TPU:0, one launch (start us, length us, event | category | flops | bytes accessed | tf_op | source)
XLA Modules:
  0.0 64.7 jit_solution(6478709204503060399)
XLA Ops:
  0.6 61.5 %shard_map.50 = (bf16[1024,2048]{1,0:T(8,128)(2,1)S(1)}, f32[128,2048]{1,0:T(8,128)S(1)}) custom-call(bf16[1024,2048]{1,0:T(8,128)(2,1)} %pre_hbm.1, bf16[2048,2048]{1,0:T(8,128)(2,1)} %w_hbm.1, bf16[1024,1024]{1,0:T(8,128)(2,1)} %cot_hbm.1), custom_call_target="tpu_custom_call" | custom-call | flops 17179869184 | bytes 41943040 | tf_op jit(solution)/shard_map/pallas_call | solution.py:517
  62.1 2.4 %shard_map.51 = (bf16[1024,2048]{1,0:T(8,128)(2,1)}, f32[128,2048]{1,0:T(8,128)}) custom-call(bf16[1024,2048]{1,0:T(8,128)(2,1)S(1)} %get-tuple-element.4.gp_in, f32[128,2048]{1,0:T(8,128)S(1)} %get-tuple-element.5.gw_in), custom_call_target="tpu_custom_call" | custom-call | flops 1 | bytes 10485760 | tf_op jit(solution)/shard_map/pallas_call | solution.py:549

commit v4 on v3

--- a/solution.py
+++ b/solution.py
@@ -15,7 +15,7 @@
 
 NEAR, FAR = (4, 4, 4, 4), (4, 4, 2, 2, 2, 2)
 CUTS = (2, 4)
-FIRST_Z, RELAYS = 0, range(8)
+FIRST_Z, RELAYS = 0, range(7)
 ORDER = (
     "n0 A0 n1 A1",
     "o4 i4 B0 n2",
@@ -34,10 +34,10 @@
     "f4 A8 B8 x5",
     "s7 t6 s8.0 x6",
     "f5 s8.1 P9 f6",
-    "A9 t7 s8.2 s8.3",
-    "B9 e0 e1 s9.0",
-    "s9.1 s9.2 s9.3 e2",
-    "e3 L0 l8 l9",
+    "A9 s8.2 s8.3 B9",
+    "e0 e1 s9.0 s9.1",
+    "s9.2 s9.3 e2 e3",
+    "L0 l7 l8 l9",
 )
 
 

time: 64.8 us -> 64.8 us (level)
  no operation moved by 1% of the time
where the time goes in v4:
time: 64.8 us; the launch traced here: 64.7 us
  Pallas kernels  63.9 us (99%)
  between operations  0.8 us (1%)
    pallas_call x1, Pallas kernels, on_device(): pl.pallas_call(functools.partial(kernel, depth, near, far, crossing, mark...  61.5 us
    pallas_call x1, Pallas kernels, on_device(): pl.pallas_call(store, out_shape=[jax.ShapeDtypeStruct((tokens, hid), BF16...  2.4 us

profile of v4, /device:TPU:0, one launch (start us, length us, event | category | flops | bytes accessed | tf_op | source)
XLA Modules:
  0.0 64.7 jit_solution(5429444935602416281)
XLA Ops:
  0.6 61.5 %shard_map.50 = (bf16[1024,2048]{1,0:T(8,128)(2,1)S(1)}, f32[128,2048]{1,0:T(8,128)S(1)}) custom-call(bf16[1024,2048]{1,0:T(8,128)(2,1)} %pre_hbm.1, bf16[2048,2048]{1,0:T(8,128)(2,1)} %w_hbm.1, bf16[1024,1024]{1,0:T(8,128)(2,1)} %cot_hbm.1), custom_call_target="tpu_custom_call" | custom-call | flops 17179869184 | bytes 41943040 | tf_op jit(solution)/shard_map/pallas_call | solution.py:517
  62.1 2.4 %shard_map.51 = (bf16[1024,2048]{1,0:T(8,128)(2,1)}, f32[128,2048]{1,0:T(8,128)}) custom-call(bf16[1024,2048]{1,0:T(8,128)(2,1)S(1)} %get-tuple-element.4.gp_in, f32[128,2048]{1,0:T(8,128)S(1)} %get-tuple-element.5.gw_in), custom_call_target="tpu_custom_call" | custom-call | flops 1 | bytes 10485760 | tf_op jit(solution)/shard_map/pallas_call | solution.py:549
